TPU v7x, 32 devices: a whole 2x2x4 slice. The times are simulated.
32 devices in a mesh: fs: 8 (over z, y), tp: 4 (over x, core).
Axes of the slice: x: 2, y: 2, z: 4, core: 2. Of those that a mesh axis runs over, the one named last changes fastest.
Arguments:
- tokens: bfloat16 [8192, 2048], P('fs', 'tp'), may hold values from -6 to 6
- mixer_gain: float32 [2048], replicated, may hold values from 0.1 to 1.9
- ffn_gain: float32 [2048], replicated, may hold values from 0.1 to 1.9
- w_outer: float32 [2048, 1024], P('fs', 'tp'), may hold values from -0.125 to 0.125
- w_inner: float32 [2048, 1024], P('fs', 'tp'), may hold values from -0.125 to 0.125
- w_value: float32 [2048, 1024], P('fs', 'tp'), may hold values from -0.125 to 0.125
- scale_outer: float32 [1, 1024], P(None, 'tp'), may hold values from 0.5 to 2
- scale_inner: float32 [1, 1024], P(None, 'tp'), may hold values from 0.5 to 2
- scale_value: float32 [1, 1024], P(None, 'tp'), may hold values from 0.5 to 2
- conv_taps: float32 [3, 1024], P(None, 'tp'), may hold values from -3.5 to 3.5
- w_mixout: float32 [1024, 2048], P('tp', 'fs'), may hold values from -0.1875 to 0.1875
- scale_mixout: float32 [1, 2048], P(None, 'fs'), may hold values from 0.5 to 2
- w_gate: float32 [2048, 5632], P('fs', 'tp'), may hold values from -0.125 to 0.125
- w_upward: float32 [2048, 5632], P('fs', 'tp'), may hold values from -0.125 to 0.125
- scale_gate: float32 [1, 5632], P(None, 'tp'), may hold values from 0.5 to 2
- scale_upward: float32 [1, 5632], P(None, 'tp'), may hold values from 0.5 to 2
- w_down: float32 [5632, 2048], P('tp', 'fs'), may hold values from -0.078125 to 0.078125
- scale_down: float32 [1, 2048], P(None, 'fs'), may hold values from 0.5 to 2
Outputs:
- block_out: bfloat16 [8192, 2048], P('fs', 'tp')
All inputs are finite; a program needn't handle non-finite values.
Results may differ from a plain program's by a relative error of at most 0.019.
Values may be sent and summed in bfloat16 or wider, within the bound.
No kernel may reach another device: no remote copies, remote signals or barrier semaphores. Data moves between devices by JAX's collectives and lax.ppermute only.
A program may use at most 128 MiB of HBM per device.

v0:
```python
import jax
import jax.numpy as jnp
from jax import lax
from jax.sharding import PartitionSpec as P

SEQ_LEN = 128


def rms_scaled(full_rows, gain_vec):
    values = full_rows.astype(jnp.float32)
    inverse = lax.rsqrt(jnp.mean(values * values, axis=-1, keepdims=True) + 1e-06)
    return (values * inverse * gain_vec).astype(jnp.bfloat16)


def add_rows(left, w_piece):
    return jnp.dot(left, w_piece, preferred_element_type=jnp.float32)


def causal_taps(product, conv_taps):
    padded = jnp.pad(product, ((0, 0), (conv_taps.shape[0] - 1, 0), (0, 0)))
    length = product.shape[1]
    summed = jnp.zeros(product.shape, jnp.float32)
    for tap_index in range(conv_taps.shape[0]):
        summed = summed + conv_taps[tap_index] * padded[:, tap_index : tap_index + length, :]
    return summed


def per_device(
    tokens,
    mixer_gain,
    ffn_gain,
    w_outer,
    w_inner,
    w_value,
    scale_outer,
    scale_inner,
    scale_value,
    conv_taps,
    w_mixout,
    scale_mixout,
    w_gate,
    w_upward,
    scale_gate,
    scale_upward,
    w_down,
    scale_down,
):
    full_rows = lax.all_gather(tokens, "tp", axis=1, tiled=True)
    normed = rms_scaled(full_rows, mixer_gain)
    tok_count = tokens.shape[0]
    local_channels = w_outer.shape[1]

    def add_one(w_piece):
        return add_rows(normed, w_piece)

    outer_bf = w_outer.astype(jnp.bfloat16)
    inner_bf = w_inner.astype(jnp.bfloat16)
    value_bf = w_value.astype(jnp.bfloat16)
    outer = add_one(lax.all_gather(outer_bf, "fs", axis=0, tiled=True))
    inner = add_one(lax.all_gather(inner_bf, "fs", axis=0, tiled=True))
    value = add_one(lax.all_gather(value_bf, "fs", axis=0, tiled=True))
    outer = outer * scale_outer
    product = inner * scale_inner * (value * scale_value)
    product = product.reshape(tok_count // SEQ_LEN, SEQ_LEN, local_channels)
    conv = causal_taps(product, conv_taps).reshape(tok_count, local_channels)
    mixed_out = (outer * conv).astype(jnp.bfloat16)
    mixout_scales, down_scales = (
        lax.all_gather(scale_mixout, "fs", axis=1, tiled=True),
        lax.all_gather(scale_down, "fs", axis=1, tiled=True),
    )
    mixout_bf = w_mixout.astype(jnp.bfloat16)
    mixed_all = lax.all_gather(mixed_out, "tp", axis=1, tiled=True)
    mixout_cols = lax.all_gather(mixout_bf, "fs", axis=1, tiled=True)
    mixout_all = lax.all_gather(mixout_cols, "tp", axis=0, tiled=True)
    mix_term = jnp.dot(mixed_all, mixout_all, preferred_element_type=jnp.float32) * mixout_scales
    residual_rows = (full_rows.astype(jnp.float32) + mix_term).astype(jnp.bfloat16)
    feature_count = tokens.shape[1]
    residual = lax.dynamic_slice_in_dim(
        residual_rows, lax.axis_index("tp") * feature_count, feature_count, 1
    )
    normed_ffn = rms_scaled(residual_rows, ffn_gain)
    gate_proj = add_rows(
        normed_ffn, lax.all_gather(w_gate.astype(jnp.bfloat16), "fs", axis=0, tiled=True)
    )
    up_proj = add_rows(
        normed_ffn, lax.all_gather(w_upward.astype(jnp.bfloat16), "fs", axis=0, tiled=True)
    )
    hidden = (jax.nn.silu(gate_proj * scale_gate) * (up_proj * scale_upward)).astype(jnp.bfloat16)
    down_terms = (
        jnp.dot(
            hidden,
            lax.all_gather(w_down.astype(jnp.bfloat16), "fs", axis=1, tiled=True),
            preferred_element_type=jnp.float32,
        )
        * down_scales
    )
    ffn_share = lax.psum_scatter(
        down_terms.astype(jnp.bfloat16), "tp", scatter_dimension=1, tiled=True
    ).astype(jnp.float32)
    return (residual.astype(jnp.float32) + ffn_share).astype(jnp.bfloat16)


def solution(mesh):
    in_specs = (
        P("fs", "tp"),
        P(),
        P(),
        P("fs", "tp"),
        P("fs", "tp"),
        P("fs", "tp"),
        P(None, "tp"),
        P(None, "tp"),
        P(None, "tp"),
        P(None, "tp"),
        P("tp", "fs"),
        P(None, "fs"),
        P("fs", "tp"),
        P("fs", "tp"),
        P(None, "tp"),
        P(None, "tp"),
        P("tp", "fs"),
        P(None, "fs"),
    )
    out_specs = P("fs", "tp")
    return jax.shard_map(
        per_device, mesh=mesh, in_specs=in_specs, out_specs=out_specs, check_vma=False
    )
```

profile of v0, /device:TPU:0, one launch (start us, length us, event | category | flops | bytes accessed | tf_op | source)
XLA Modules:
  0.0 623.6 jit_solution(6061713341310638662)
XLA Ops:
  6.5 1.6 convert_element_type.63
  8.2 0.0 all-gather.21.cloned.1.call-update
  8.2 0.0 all-gather.11.cloned.1.call-start
  8.2 0.7 all-gather.11.cloned.1.call-update
  8.9 0.0 all-gather.17.cloned.1.call-start
  9.0 1.6 convert_element_type.61
  10.6 0.0 all-gather.15.cloned.1.call-start
  10.7 1.6 convert_element_type.60
  12.3 0.0 all-gather.15.cloned.1.call-update
  12.3 0.0 all-gather.13.cloned.1.call-start
  12.4 1.6 convert_element_type.59
  14.0 0.0 all-gather.23.cloned.1.call-start
  14.0 37.5 %all-gather.21.cloned.1.call-done = bf16[256,2048]{1,0:T(8,128)(2,1)} async-done(((bf16[256,256]{1,0:T(8,128)(2,1)}), bf16[256,2048]{1,0:T(8,128)(2,1)}) %all-gather.21.cloned.1.call-update) | async-done | bytes 1048592 | tf_op jit(solution)/shard_map/all_gather | solution.py:73
  51.5 0.0 all-gather.23.cloned.1.call-update
  51.6 0.0 all-gather.19.cloned.1.call-start
  51.6 0.8 fusion.20
  52.4 34.2 %all-gather.11.cloned.1.call-done = bf16[1024,2048]{1,0:T(8,128)(2,1)} async-done(((bf16[1024,512]{1,0:T(8,128)(2,1)}), bf16[1024,2048]{1,0:T(8,128)(2,1)}) %all-gather.11.cloned.1.call-update) | async-done | bytes 4194320 | tf_op jit(solution)/shard_map/all_gather | solution.py:48
  86.6 3.1 fusion.3
  89.7 39.4 %all-gather.17.cloned.1.call-done = bf16[2048,256]{1,0:T(8,128)(2,1)} async-done(((bf16[256,256]{1,0:T(8,128)(2,1)}), bf16[2048,256]{1,0:T(8,128)(2,1)}) %all-gather.17.cloned.1.call-update) | async-done | bytes 1048592 | tf_op jit(solution)/shard_map/all_gather | solution.py:61
  129.0 3.8 convolution_multiply_fusion
  132.9 37.2 %all-gather.15.cloned.1.call-done = bf16[2048,256]{1,0:T(8,128)(2,1)} async-done(((bf16[256,256]{1,0:T(8,128)(2,1)}), bf16[2048,256]{1,0:T(8,128)(2,1)}) %all-gather.15.cloned.1.call-update) | async-done | bytes 1048592 | tf_op jit(solution)/shard_map/all_gather | solution.py:60
  170.0 3.8 fusion.8
  173.9 1.3 fusion.15
  175.2 35.9 %all-gather.13.cloned.1.call-done = bf16[2048,256]{1,0:T(8,128)(2,1)} async-done(((bf16[256,256]{1,0:T(8,128)(2,1)}), bf16[2048,256]{1,0:T(8,128)(2,1)}) %all-gather.13.cloned.1.call-update) | async-done | bytes 1048592 | tf_op jit(solution)/shard_map/all_gather | solution.py:59
  211.0 5.1 fusion.9
  216.1 0.0 all-gather.19.cloned.1.call-update
  216.2 0.0 all-gather.25.cloned.1.call-start
  216.2 1.0 convert_element_type.68
  217.2 0.0 all-gather.25.cloned.1.call-update
  217.2 0.0 all-gather.27.cloned.1.call-start
  217.3 1.0 convert_element_type.69
  218.2 0.0 all-gather.27.cloned.1.call-update
  218.3 0.0 all-gather.29.cloned.1.call-start
  218.3 2.5 convert_element_type.71
  220.8 0.0 all-gather.29.cloned.1.call-update
  220.8 0.0 reduce-scatter.2.cloned.1.call-start
  220.9 18.2 %all_gather.43 = f32[1,2048]{1,0:T(1,128)S(1)} all-gather(f32[1,256]{1,0:T(1,128)S(1)} %copy-done.4), channel_id=1, replica_groups=mesh['fs'=8,'tp'=4] {'fs'}, dimensions={1}, use_global_device_ids=true | all-gather | bytes 9216 | tf_op jit(solution)/shard_map/all_gather | solution.py:68
  239.1 16.6 %all_gather.47 = f32[1,2048]{1,0:T(1,128)S(1)} all-gather(f32[1,256]{1,0:T(1,128)S(1)} %copy-done.5), channel_id=1, replica_groups=mesh['fs'=8,'tp'=4] {'fs'}, dimensions={1}, use_global_device_ids=true | all-gather | bytes 9216 | tf_op jit(solution)/shard_map/all_gather | solution.py:69
  255.7 14.3 %all-gather.19.cloned.1.call-done = bf16[1024,1024]{1,0:T(8,128)(2,1)} async-done(((bf16[1024,256]{1,0:T(8,128)(2,1)}), bf16[1024,1024]{1,0:T(8,128)(2,1)}) %all-gather.19.cloned.1.call-update) | async-done | bytes 2097168 | tf_op jit(solution)/shard_map/all_gather | solution.py:72
  270.1 10.9 %fusion = (f32[1024]{0:T(1024)S(1)}, bf16[1024,2048]{1,0:T(8,128)(2,1)}) fusion(f32[2048]{0:T(1024)S(1)} %bitcast.26, bf16[1024,1024]{1,0:T(8,128)(2,1)} %all-gather.19.cloned.1.call-done, bf16[1024,2048]{1,0:T(8,128)(2,1)} %all-gather.23.cloned.1.call-done, bf16[1024,2048]{1,0:T(8,128)(2,1)} %all-gather.11.cloned.1.call-done), kind=kOutput, calls=%fused_computation.5 | convolution fusion | flops 4309646336 | bytes 14692352 | tf_op jit(solution)/shard_map/dot_general | solution.py:75
  281.0 83.6 %all-gather.25.cloned.1.call-done = bf16[2048,1408]{1,0:T(8,128)(2,1)} async-done(((bf16[256,1408]{1,0:T(8,128)(2,1)}), bf16[2048,1408]{1,0:T(8,128)(2,1)}) %all-gather.25.cloned.1.call-update) | async-done | bytes 5767184 | tf_op jit(solution)/shard_map/all_gather | solution.py:83
  364.6 11.9 %fusion.11 = f32[1024,1408]{1,0:T(8,128)} fusion(bf16[2048,1408]{1,0:T(8,128)(2,1)} %all-gather.25.cloned.1.call-done, bf16[1024,2048]{1,0:T(8,128)(2,1)} %get-tuple-element.9, f32[2048]{0:T(1024)S(1)} %copy-done.7, f32[1024]{0:T(1024)S(1)} %add_rsqrt_fusion), kind=kOutput, calls=%fused_computation.21 | convolution fusion | flops 5913968640 | bytes 15740928 | tf_op jit(solution)/shard_map/dot_general | solution.py:16
  376.5 80.8 %all-gather.27.cloned.1.call-done = bf16[2048,1408]{1,0:T(8,128)(2,1)} async-done(((bf16[256,1408]{1,0:T(8,128)(2,1)}), bf16[2048,1408]{1,0:T(8,128)(2,1)}) %all-gather.27.cloned.1.call-update) | async-done | bytes 5767184 | tf_op jit(solution)/shard_map/all_gather | solution.py:86
  457.3 93.2 %all-gather.29.cloned.1.call-done = bf16[1408,2048]{1,0:T(8,128)(2,1)} async-done(((bf16[1408,256]{1,0:T(8,128)(2,1)}), bf16[1408,2048]{1,0:T(8,128)(2,1)}) %all-gather.29.cloned.1.call-update) | async-done | bytes 5767184 | tf_op jit(solution)/shard_map/all_gather | solution.py:92
  550.5 21.0 %multiply_convert_fusion = bf16[1024,2048]{1,0:T(8,128)(2,1)} fusion(bf16[1408,2048]{1,0:T(8,128)(2,1)} %all-gather.29.cloned.1.call-done, f32[2048]{0:T(1024)S(1)} %bitcast.25, f32[1024,1408]{1,0:T(8,128)} %fusion.11, bf16[2048,1408]{1,0:T(8,128)(2,1)} %all-gather.27.cloned.1.call-done, f32[1408]{0:T(1024)S(1)} %reduce.1, f32[1408]{0:T(1024)S(1)} %reduce, ...), kind=kOutput, calls=%fused_computation.12 | convolution fusion | flops 11835277312 | bytes 25721856 | tf_op jit(solution)/shard_map/dot_general | solution.py:90
  571.5 0.0 reduce-scatter.2.cloned.1.call-update
  571.6 42.7 %reduce-scatter.2.cloned.1.call-done = bf16[1024,512]{1,0:T(8,128)(2,1)} async-done(((bf16[1024,2048]{1,0:T(8,128)(2,1)}), bf16[1024,512]{1,0:T(8,128)(2,1)}) %reduce-scatter.2.cloned.1.call-update) | async-done | bytes 1048592 | tf_op jit(solution)/shard_map/reduce_scatter | solution.py:97
  614.3 2.8 add_convert_fusion
  (30 shorter events, 0.1 us)
Async XLA Ops:
  6.5 122.5 %copy-start.8 = (f32[1,256]{1,0:T(1,128)S(1)}, f32[1,256]{1,0:T(1,128)}, u32[]{:S(2)}) copy-start(f32[1,256]{1,0:T(1,128)} %param.26) | copy-start | bytes 3076
  6.5 122.5 %copy-start.6 = (f32[2048]{0:T(1024)S(1)}, f32[2048]{0:T(1024)}, u32[]{:S(2)}) copy-start(f32[2048]{0:T(1024)} %param.19) | copy-start | bytes 24580
  6.5 45.0 %all-gather.21.cloned.1.call-start = ((), (), s32[]{:S(2)}) async-start(), calls=%async_computation.6 | async-start | bytes 1179648 | tf_op jit(solution)/shard_map/all_gather | solution.py:73
  8.2 78.4 %all-gather.11.cloned.1.call-start = ((), (), s32[]{:S(2)}) async-start(), calls=%async_computation.1 | async-start | bytes 5242880 | tf_op jit(solution)/shard_map/all_gather | solution.py:48
  8.9 120.1 %all-gather.17.cloned.1.call-start = ((), (), s32[]{:S(2)}) async-start(), calls=%async_computation.4 | async-start | bytes 1179648 | tf_op jit(solution)/shard_map/all_gather | solution.py:61
  10.6 159.4 %all-gather.15.cloned.1.call-start = ((), (), s32[]{:S(2)}) async-start(), calls=%async_computation.3 | async-start | bytes 1179648 | tf_op jit(solution)/shard_map/all_gather | solution.py:60
  12.3 198.7 %all-gather.13.cloned.1.call-start = ((), (), s32[]{:S(2)}) async-start(), calls=%async_computation.2 | async-start | bytes 1179648 | tf_op jit(solution)/shard_map/all_gather | solution.py:59
  14.0 241.7 %all-gather.23.cloned.1.call-start = ((), (), s32[]{:S(2)}) async-start(), calls=%async_computation.7 | async-start | bytes 5242880 | tf_op jit(solution)/shard_map/all_gather | solution.py:74
  51.6 218.5 %all-gather.19.cloned.1.call-start = ((), (), s32[]{:S(2)}) async-start(), calls=%async_computation.5 | async-start | bytes 2621440 | tf_op jit(solution)/shard_map/all_gather | solution.py:72
  129.0 41.0 %copy-start.9 = (f32[1,256]{1,0:T(1,128)S(1)}, f32[1,256]{1,0:T(1,128)}, u32[]{:S(2)}) copy-start(f32[1,256]{1,0:T(1,128)} %param.25) | copy-start | bytes 3076
  170.0 41.0 %copy-start.10 = (f32[1,256]{1,0:T(1,128)S(1)}, f32[1,256]{1,0:T(1,128)}, u32[]{:S(2)}) copy-start(f32[1,256]{1,0:T(1,128)} %param.24) | copy-start | bytes 3076
  211.0 5.2 copy-start
  211.0 6.2 copy-start.1
  216.1 4.7 copy-start.2
  216.1 4.8 copy-start.3
  216.1 4.8 copy-start.4
  216.1 23.0 %copy-start.5 = (f32[1,256]{1,0:T(1,128)S(1)}, f32[1,256]{1,0:T(1,128)}, u32[]{:S(2)}) copy-start(f32[1,256]{1,0:T(1,128)} %param.35) | copy-start | bytes 3076
  216.2 148.4 %all-gather.25.cloned.1.call-start = ((), (), s32[]{:S(2)}) async-start(), calls=%async_computation.8 | async-start | bytes 6488064 | tf_op jit(solution)/shard_map/all_gather | solution.py:83
  217.2 240.1 %all-gather.27.cloned.1.call-start = ((), (), s32[]{:S(2)}) async-start(), calls=%async_computation.9 | async-start | bytes 6488064 | tf_op jit(solution)/shard_map/all_gather | solution.py:86
  218.3 332.3 %all-gather.29.cloned.1.call-start = ((), (), s32[]{:S(2)}) async-start(), calls=%async_computation.10 | async-start | bytes 6488064 | tf_op jit(solution)/shard_map/all_gather | solution.py:92
  220.8 393.5 %reduce-scatter.2.cloned.1.call-start = ((), (), s32[]{:S(2)}) async-start(), calls=%async_computation.11 | async-start | bytes 5242880 | tf_op jit(solution)/shard_map/reduce_scatter | solution.py:97
  270.0 94.5 %copy-start.7 = (f32[2048]{0:T(1024)S(1)}, f32[2048]{0:T(1024)}, u32[]{:S(2)}) copy-start(f32[2048]{0:T(1024)} %param.20) | copy-start | bytes 24580
Sparse Core Ops, SparseCore 0:
  9.4 42.1 all-gather.20
  53.1 33.4 all-gather.10
  88.7 40.2 all-gather.16
  131.0 38.9 all-gather.14
  172.0 38.9 all-gather.12
  212.5 33.1 all-gather.22
  247.2 22.8 all-gather.18
  272.2 92.2 all-gather.24
  366.8 90.4 all-gather.26
  459.2 91.2 all-gather.28
  571.7 42.5 reduce-scatter.1
where the time goes:
time: 624 us
  waiting for transfers between devices  500 us (80%)
  matrix products  56.6 us (9%)
  blocking collectives  34.8 us (6%)
  other arithmetic  18 us (3%)
  between operations  13.3 us (2%)
    all_gather x1, waiting for transfers between devices, per_device(): lax.all_gather(w_down.astype(jnp.bfloat16), 'fs', axis=1, tiled=True)  93.2 us
    all_gather x1, waiting for transfers between devices, per_device(): lax.all_gather(w_gate.astype(jnp.bfloat16), 'fs', axis=0, tiled=True)  83.6 us
    all_gather x1, waiting for transfers between devices, per_device(): lax.all_gather(w_upward.astype(jnp.bfloat16), 'fs', axis=0, tiled=True)  80.8 us
    reduce_scatter x1, waiting for transfers between devices, per_device(): lax.psum_scatter(down_terms.astype(jnp.bfloat16), 'tp', scatter_dimension...  42.7 us
    all_gather x1, waiting for transfers between devices, per_device(): value = add_one(lax.all_gather(value_bf, 'fs', axis=0, tiled=True))  39.4 us
    all_gather x1, waiting for transfers between devices, per_device(): mixout_cols = lax.all_gather(mixout_bf, 'fs', axis=1, tiled=True)  37.5 us
    all_gather x1, waiting for transfers between devices, per_device(): inner = add_one(lax.all_gather(inner_bf, 'fs', axis=0, tiled=True))  37.2 us
    all_gather x1, waiting for transfers between devices, per_device(): outer = add_one(lax.all_gather(outer_bf, 'fs', axis=0, tiled=True))  35.9 us
  transfers between devices with their start and end apart: 11, of which 10 were waited for; matrix products, arithmetic and copies ran while one was open for 8% of the time, Pallas kernels for 0%

commit v1 on v0

--- a/solution.py
+++ b/solution.py
@@ -70,7 +70,12 @@
     )
     mixout_bf = w_mixout.astype(jnp.bfloat16)
     mixed_all = lax.all_gather(mixed_out, "tp", axis=1, tiled=True)
-    mixout_cols = lax.all_gather(mixout_bf, "fs", axis=1, tiled=True)
+    ring = [mixout_bf]
+    for hop in range(7):
+        ring.append(lax.ppermute(ring[-1], "fs", [(dev, (dev + 1) % 8) for dev in range(8)]))
+    mixout_cols = jnp.roll(
+        jnp.concatenate(ring[::-1], axis=1), (lax.axis_index("fs") + 1) * ring[0].shape[1], axis=1
+    )
     mixout_all = lax.all_gather(mixout_cols, "tp", axis=0, tiled=True)
     mix_term = jnp.dot(mixed_all, mixout_all, preferred_element_type=jnp.float32) * mixout_scales
     residual_rows = (full_rows.astype(jnp.float32) + mix_term).astype(jnp.bfloat16)

time: 624 us -> 585 us (0.938)
  waiting for transfers between devices: 500 us -> 459 us
    ppermute x0 -> x7, waiting for transfers between devices: none -> 52.5 us  [per_device(): lax.ppermute(ring[-1], 'fs', [(dev, (dev + 1) % 8) for dev in range(8)])]
    all_gather x1 -> x0, waiting for transfers between devices: 37.5 us -> none  [per_device(): mixout_cols = lax.all_gather(mixout_bf, 'fs', axis=1, tiled=True)]
    all_gather x1, waiting for transfers between devices: 34.2 us -> 0.02 us  [per_device(): full_rows = lax.all_gather(tokens, 'tp', axis=1, tiled=True)]
    all_gather x1, waiting for transfers between devices: 39.4 us -> 15.6 us  [per_device(): value = add_one(lax.all_gather(value_bf, 'fs', axis=0, tiled=True))]
  transfers between devices with their start and end apart: 11 -> 17, of which waited for: 10 -> 15; matrix products, arithmetic and copies ran while one was open for 8% -> 8% of each run, Pallas kernels for 0% -> 0%
where the time goes in v1:
time: 585 us; the launch traced here: 584 us
  waiting for transfers between devices  459 us (78%)
  matrix products  56.2 us (10%)
  blocking collectives  34.8 us (6%)
  other arithmetic  15 us (3%)
  between operations  13.9 us (2%)
    all_gather x1, waiting for transfers between devices, per_device(): lax.all_gather(w_down.astype(jnp.bfloat16), 'fs', axis=1, tiled=True)  93.4 us
    all_gather x1, waiting for transfers between devices, per_device(): lax.all_gather(w_gate.astype(jnp.bfloat16), 'fs', axis=0, tiled=True)  83.6 us
    all_gather x1, waiting for transfers between devices, per_device(): lax.all_gather(w_upward.astype(jnp.bfloat16), 'fs', axis=0, tiled=True)  80.7 us
    ppermute x7, waiting for transfers between devices, per_device(): lax.ppermute(ring[-1], 'fs', [(dev, (dev + 1) % 8) for dev in range(8)])  52.5 us
    reduce_scatter x1, waiting for transfers between devices, per_device(): lax.psum_scatter(down_terms.astype(jnp.bfloat16), 'tp', scatter_dimension...  42.7 us
    all_gather x1, waiting for transfers between devices, per_device(): inner = add_one(lax.all_gather(inner_bf, 'fs', axis=0, tiled=True))  37.3 us
    all_gather x1, waiting for transfers between devices, per_device(): outer = add_one(lax.all_gather(outer_bf, 'fs', axis=0, tiled=True))  36.8 us
    dot_general x4, matrix products, add_rows(): return jnp.dot(left, w_piece, preferred_element_type=jnp.float32)  24.3 us
  transfers between devices with their start and end apart: 17, of which 15 were waited for; matrix products, arithmetic and copies ran while one was open for 8% of the time, Pallas kernels for 0%

profile of v1, /device:TPU:0, one launch (start us, length us, event | category | flops | bytes accessed | tf_op | source)
XLA Modules:
  0.0 584.2 jit_solution(13378560600639885881)
XLA Ops:
  6.5 0.7 all-gather.10.cloned.1.call-update
  7.3 0.0 all-gather.16.cloned.1.call-start
  7.3 1.6 convert_element_type.61
  8.9 0.0 all-gather.16.cloned.1.call-update
  8.9 0.0 all-gather.14.cloned.1.call-start
  9.0 1.6 convert_element_type.60
  10.6 0.0 all-gather.12.cloned.1.call-start
  10.7 1.0 convert_element_type.63
  11.7 3.0 collective-permute-start
  14.7 6.5 %collective-permute-done = bf16[256,256]{1,0:T(8,128)(2,1)S(1)} collective-permute-done((bf16[256,256]{1,0:T(8,128)(2,1)S(1)}, bf16[256,256]{1,0:T(8,128)(2,1)S(1)}, u32[]{:S(2)}, u32[]{:S(2)}) %collective-permute-start) | collective-permute-done | bytes 131104 | tf_op jit(solution)/shard_map/ppermute | solution.py:75
  21.2 7.7 %collective-permute-done.1 = bf16[256,256]{1,0:T(8,128)(2,1)S(1)} collective-permute-done((bf16[256,256]{1,0:T(8,128)(2,1)S(1)}, bf16[256,256]{1,0:T(8,128)(2,1)S(1)}, u32[]{:S(2)}, u32[]{:S(2)}) %collective-permute-start.1) | collective-permute-done | bytes 131104 | tf_op jit(solution)/shard_map/ppermute | solution.py:75
  28.9 7.7 %collective-permute-done.2 = bf16[256,256]{1,0:T(8,128)(2,1)S(1)} collective-permute-done((bf16[256,256]{1,0:T(8,128)(2,1)S(1)}, bf16[256,256]{1,0:T(8,128)(2,1)S(1)}, u32[]{:S(2)}, u32[]{:S(2)}) %collective-permute-start.2) | collective-permute-done | bytes 131104 | tf_op jit(solution)/shard_map/ppermute | solution.py:75
  36.6 7.7 %collective-permute-done.3 = bf16[256,256]{1,0:T(8,128)(2,1)S(1)} collective-permute-done((bf16[256,256]{1,0:T(8,128)(2,1)S(1)}, bf16[256,256]{1,0:T(8,128)(2,1)S(1)}, u32[]{:S(2)}, u32[]{:S(2)}) %collective-permute-start.3) | collective-permute-done | bytes 131104 | tf_op jit(solution)/shard_map/ppermute | solution.py:75
  44.2 7.7 %collective-permute-done.4 = bf16[256,256]{1,0:T(8,128)(2,1)S(1)} collective-permute-done((bf16[256,256]{1,0:T(8,128)(2,1)S(1)}, bf16[256,256]{1,0:T(8,128)(2,1)S(1)}, u32[]{:S(2)}, u32[]{:S(2)}) %collective-permute-start.4) | collective-permute-done | bytes 131104 | tf_op jit(solution)/shard_map/ppermute | solution.py:75
  51.9 9.0 %collective-permute-done.5 = bf16[256,256]{1,0:T(8,128)(2,1)S(1)} collective-permute-done((bf16[256,256]{1,0:T(8,128)(2,1)S(1)}, bf16[256,256]{1,0:T(8,128)(2,1)S(1)}, u32[]{:S(2)}, u32[]{:S(2)}) %collective-permute-start.5) | collective-permute-done | bytes 131104 | tf_op jit(solution)/shard_map/ppermute | solution.py:75
  60.9 1.6 convert_element_type.59
  62.6 0.0 all-gather.20.cloned.1.call-start
  62.6 6.3 %collective-permute-done.6 = bf16[256,256]{1,0:T(8,128)(2,1)S(1)} collective-permute-done((bf16[256,256]{1,0:T(8,128)(2,1)S(1)}, bf16[256,256]{1,0:T(8,128)(2,1)S(1)}, u32[]{:S(2)}, u32[]{:S(2)}) %collective-permute-start.6) | collective-permute-done | bytes 131104 | tf_op jit(solution)/shard_map/ppermute | solution.py:75
  69.3 1.0 constant_dynamic-slice_fusion
  70.3 0.0 all-gather.18.cloned.1.call-start
  70.4 0.0 all-gather.10.cloned.1.call-done
  70.5 3.1 fusion.3
  73.5 15.6 %all-gather.16.cloned.1.call-done = bf16[2048,256]{1,0:T(8,128)(2,1)} async-done(((bf16[256,256]{1,0:T(8,128)(2,1)}), bf16[2048,256]{1,0:T(8,128)(2,1)}) %all-gather.16.cloned.1.call-update) | async-done | bytes 1048592 | tf_op jit(solution)/shard_map/all_gather | solution.py:61
  89.2 3.8 convolution_multiply_fusion
  93.0 37.3 %all-gather.14.cloned.1.call-done = bf16[2048,256]{1,0:T(8,128)(2,1)} async-done(((bf16[256,256]{1,0:T(8,128)(2,1)}), bf16[2048,256]{1,0:T(8,128)(2,1)}) %all-gather.14.cloned.1.call-update) | async-done | bytes 1048592 | tf_op jit(solution)/shard_map/all_gather | solution.py:60
  130.3 3.8 fusion.8
  134.1 0.3 fusion.15
  134.5 36.8 %all-gather.12.cloned.1.call-done = bf16[2048,256]{1,0:T(8,128)(2,1)} async-done(((bf16[256,256]{1,0:T(8,128)(2,1)}), bf16[2048,256]{1,0:T(8,128)(2,1)}) %all-gather.12.cloned.1.call-update) | async-done | bytes 1048592 | tf_op jit(solution)/shard_map/all_gather | solution.py:59
  171.3 4.7 fusion.9
  176.1 0.0 all-gather.22.cloned.1.call-start
  176.2 1.0 convert_element_type.68
  177.2 0.0 all-gather.24.cloned.1.call-start
  177.2 0.5 copy-done.2
  177.7 1.0 convert_element_type.69
  178.7 0.0 all-gather.26.cloned.1.call-start
  178.7 1.0 convert_element_type.71
  179.7 0.0 reduce-scatter.2.cloned.1.call-start
  179.9 18.3 %all_gather.39 = f32[1,2048]{1,0:T(1,128)S(1)} all-gather(f32[1,256]{1,0:T(1,128)S(1)} %copy-done.7), channel_id=1, replica_groups=mesh['fs'=8,'tp'=4] {'fs'}, dimensions={1}, use_global_device_ids=true | all-gather | bytes 9216 | tf_op jit(solution)/shard_map/all_gather | solution.py:68
  198.1 16.5 %all_gather.43 = f32[1,2048]{1,0:T(1,128)S(1)} all-gather(f32[1,256]{1,0:T(1,128)S(1)} %copy-done.8), channel_id=1, replica_groups=mesh['fs'=8,'tp'=4] {'fs'}, dimensions={1}, use_global_device_ids=true | all-gather | bytes 9216 | tf_op jit(solution)/shard_map/all_gather | solution.py:69
  214.6 15.5 %all-gather.18.cloned.1.call-done = bf16[1024,1024]{1,0:T(8,128)(2,1)} async-done(((bf16[1024,256]{1,0:T(8,128)(2,1)}), bf16[1024,1024]{1,0:T(8,128)(2,1)}) %all-gather.18.cloned.1.call-update) | async-done | bytes 2097168 | tf_op jit(solution)/shard_map/all_gather | solution.py:72
  230.2 10.9 %fusion = (f32[1024]{0:T(1024)S(1)}, bf16[1024,2048]{1,0:T(8,128)(2,1)}) fusion(f32[2048]{0:T(1024)S(1)} %bitcast.26, bf16[1024,1024]{1,0:T(8,128)(2,1)} %all-gather.18.cloned.1.call-done, bf16[1024,2048]{1,0:T(8,128)(2,1)} %all-gather.20.cloned.1.call-done, bf16[1024,2048]{1,0:T(8,128)(2,1)} %all-gather.10.cloned.1.call-done), kind=kOutput, calls=%fused_computation.5 | convolution fusion | flops 4309646336 | bytes 14692352 | tf_op jit(solution)/shard_map/dot_general | solution.py:80
  241.1 83.6 %all-gather.22.cloned.1.call-done = bf16[2048,1408]{1,0:T(8,128)(2,1)} async-done(((bf16[256,1408]{1,0:T(8,128)(2,1)}), bf16[2048,1408]{1,0:T(8,128)(2,1)}) %all-gather.22.cloned.1.call-update) | async-done | bytes 5767184 | tf_op jit(solution)/shard_map/all_gather | solution.py:88
  324.7 12.0 %fusion.11 = f32[1024,1408]{1,0:T(8,128)} fusion(bf16[2048,1408]{1,0:T(8,128)(2,1)} %all-gather.22.cloned.1.call-done, bf16[1024,2048]{1,0:T(8,128)(2,1)} %get-tuple-element.9, f32[2048]{0:T(1024)S(1)} %copy-done.10, f32[1024]{0:T(1024)S(1)} %add_rsqrt_fusion), kind=kOutput, calls=%fused_computation.21 | convolution fusion | flops 5913968640 | bytes 15740928 | tf_op jit(solution)/shard_map/dot_general | solution.py:16
  336.6 80.7 %all-gather.24.cloned.1.call-done = bf16[2048,1408]{1,0:T(8,128)(2,1)} async-done(((bf16[256,1408]{1,0:T(8,128)(2,1)}), bf16[2048,1408]{1,0:T(8,128)(2,1)}) %all-gather.24.cloned.1.call-update) | async-done | bytes 5767184 | tf_op jit(solution)/shard_map/all_gather | solution.py:91
  417.4 93.4 %all-gather.26.cloned.1.call-done = bf16[1408,2048]{1,0:T(8,128)(2,1)} async-done(((bf16[1408,256]{1,0:T(8,128)(2,1)}), bf16[1408,2048]{1,0:T(8,128)(2,1)}) %all-gather.26.cloned.1.call-update) | async-done | bytes 5767184 | tf_op jit(solution)/shard_map/all_gather | solution.py:97
  510.8 21.0 %multiply_convert_fusion = bf16[1024,2048]{1,0:T(8,128)(2,1)} fusion(bf16[1408,2048]{1,0:T(8,128)(2,1)} %all-gather.26.cloned.1.call-done, f32[2048]{0:T(1024)S(1)} %bitcast.25, f32[1024,1408]{1,0:T(8,128)} %fusion.11, bf16[2048,1408]{1,0:T(8,128)(2,1)} %all-gather.24.cloned.1.call-done, f32[1408]{0:T(1024)S(1)} %reduce.1, f32[1408]{0:T(1024)S(1)} %reduce, ...), kind=kOutput, calls=%fused_computation.12 | convolution fusion | flops 11835277312 | bytes 25721856 | tf_op jit(solution)/shard_map/dot_general | solution.py:95
  531.8 42.7 %reduce-scatter.2.cloned.1.call-done = bf16[1024,512]{1,0:T(8,128)(2,1)} async-done(((bf16[1024,2048]{1,0:T(8,128)(2,1)}), bf16[1024,512]{1,0:T(8,128)(2,1)}) %reduce-scatter.2.cloned.1.call-update) | async-done | bytes 1048592 | tf_op jit(solution)/shard_map/reduce_scatter | solution.py:102
  574.5 2.8 add_convert_fusion
  (64 shorter events, 0.5 us)
Async XLA Ops:
  6.5 62.5 %copy-start = (f32[256,256]{1,0:T(8,128)S(1)}, f32[256,256]{1,0:T(8,128)}, u32[]{:S(2)}) copy-start(f32[256,256]{1,0:T(8,128)} %param.28) | copy-start | bytes 786436
  6.5 63.9 %all-gather.10.cloned.1.call-start = ((), (), s32[]{:S(2)}) async-start(), calls=%async_computation.1 | async-start | bytes 5242880 | tf_op jit(solution)/shard_map/all_gather | solution.py:48
  7.3 81.9 %all-gather.16.cloned.1.call-start = ((), (), s32[]{:S(2)}) async-start(), calls=%async_computation.4 | async-start | bytes 1179648 | tf_op jit(solution)/shard_map/all_gather | solution.py:61
  8.9 121.4 %all-gather.14.cloned.1.call-start = ((), (), s32[]{:S(2)}) async-start(), calls=%async_computation.3 | async-start | bytes 1179648 | tf_op jit(solution)/shard_map/all_gather | solution.py:60
  10.6 59.8 %copy-start.6 = (f32[3,256]{1,0:T(4,128)S(1)}, f32[3,256]{1,0:T(4,128)}, u32[]{:S(2)}) copy-start(f32[3,256]{1,0:T(4,128)} %param.27) | copy-start | bytes 9220
  10.6 160.7 %all-gather.12.cloned.1.call-start = ((), (), s32[]{:S(2)}) async-start(), calls=%async_computation.2 | async-start | bytes 1179648 | tf_op jit(solution)/shard_map/all_gather | solution.py:59
  11.7 9.6 %collective-permute-start = (bf16[256,256]{1,0:T(8,128)(2,1)S(1)}, bf16[256,256]{1,0:T(8,128)(2,1)S(1)}, u32[]{:S(2)}, u32[]{:S(2)}) collective-permute-start(bf16[256,256]{1,0:T(8,128)(2,1)S(1)} %convert_element_type.63), channel_id=1, source_target_pairs={{0,4},{4,8},{8,12},{12,16},{16,20},{20,24},{24,28},{28,0},{1,5},{5... | collective-permute-start | bytes 393224 | tf_op jit(solution)/shard_map/ppermute | solution.py:75
  21.2 7.7 %collective-permute-start.1 = (bf16[256,256]{1,0:T(8,128)(2,1)S(1)}, bf16[256,256]{1,0:T(8,128)(2,1)S(1)}, u32[]{:S(2)}, u32[]{:S(2)}) collective-permute-start(bf16[256,256]{1,0:T(8,128)(2,1)S(1)} %collective-permute-done), channel_id=1, source_target_pairs={{0,4},{4,8},{8,12},{12,16},{16,20},{20,24},{24,28},{28,0},{1,5},{5... | collective-permute-start | bytes 393224 | tf_op jit(solution)/shard_map/ppermute | solution.py:75
  28.9 7.7 %collective-permute-start.2 = (bf16[256,256]{1,0:T(8,128)(2,1)S(1)}, bf16[256,256]{1,0:T(8,128)(2,1)S(1)}, u32[]{:S(2)}, u32[]{:S(2)}) collective-permute-start(bf16[256,256]{1,0:T(8,128)(2,1)S(1)} %collective-permute-done.1), channel_id=1, source_target_pairs={{0,4},{4,8},{8,12},{12,16},{16,20},{20,24},{24,28},{28,0},{1,5},{5... | collective-permute-start | bytes 393224 | tf_op jit(solution)/shard_map/ppermute | solution.py:75
  36.6 7.7 %collective-permute-start.3 = (bf16[256,256]{1,0:T(8,128)(2,1)S(1)}, bf16[256,256]{1,0:T(8,128)(2,1)S(1)}, u32[]{:S(2)}, u32[]{:S(2)}) collective-permute-start(bf16[256,256]{1,0:T(8,128)(2,1)S(1)} %collective-permute-done.2), channel_id=1, source_target_pairs={{0,4},{4,8},{8,12},{12,16},{16,20},{20,24},{24,28},{28,0},{1,5},{5... | collective-permute-start | bytes 393224 | tf_op jit(solution)/shard_map/ppermute | solution.py:75
  44.2 7.7 %collective-permute-start.4 = (bf16[256,256]{1,0:T(8,128)(2,1)S(1)}, bf16[256,256]{1,0:T(8,128)(2,1)S(1)}, u32[]{:S(2)}, u32[]{:S(2)}) collective-permute-start(bf16[256,256]{1,0:T(8,128)(2,1)S(1)} %collective-permute-done.3), channel_id=1, source_target_pairs={{0,4},{4,8},{8,12},{12,16},{16,20},{20,24},{24,28},{28,0},{1,5},{5... | collective-permute-start | bytes 393224 | tf_op jit(solution)/shard_map/ppermute | solution.py:75
  51.9 9.0 %collective-permute-start.5 = (bf16[256,256]{1,0:T(8,128)(2,1)S(1)}, bf16[256,256]{1,0:T(8,128)(2,1)S(1)}, u32[]{:S(2)}, u32[]{:S(2)}) collective-permute-start(bf16[256,256]{1,0:T(8,128)(2,1)S(1)} %collective-permute-done.4), channel_id=1, source_target_pairs={{0,4},{4,8},{8,12},{12,16},{16,20},{20,24},{24,28},{28,0},{1,5},{5... | collective-permute-start | bytes 393224 | tf_op jit(solution)/shard_map/ppermute | solution.py:75
  60.9 8.0 %collective-permute-start.6 = (bf16[256,256]{1,0:T(8,128)(2,1)S(1)}, bf16[256,256]{1,0:T(8,128)(2,1)S(1)}, u32[]{:S(2)}, u32[]{:S(2)}) collective-permute-start(bf16[256,256]{1,0:T(8,128)(2,1)S(1)} %collective-permute-done.5), channel_id=1, source_target_pairs={{0,4},{4,8},{8,12},{12,16},{16,20},{20,24},{24,28},{28,0},{1,5},{5... | collective-permute-start | bytes 393224 | tf_op jit(solution)/shard_map/ppermute | solution.py:75
  62.6 152.1 %all-gather.20.cloned.1.call-start = ((), (), s32[]{:S(2)}) async-start(), calls=%async_computation.6 | async-start | bytes 5242880 | tf_op jit(solution)/shard_map/all_gather | solution.py:79
  69.2 20.0 %copy-start.9 = (f32[2048]{0:T(1024)S(1)}, f32[2048]{0:T(1024)}, u32[]{:S(2)}) copy-start(f32[2048]{0:T(1024)} %param.19) | copy-start | bytes 24580
  69.2 19.9 %copy-start.11 = (f32[1,256]{1,0:T(1,128)S(1)}, f32[1,256]{1,0:T(1,128)}, u32[]{:S(2)}) copy-start(f32[1,256]{1,0:T(1,128)} %param.26) | copy-start | bytes 3076
  70.3 159.8 %all-gather.18.cloned.1.call-start = ((), (), s32[]{:S(2)}) async-start(), calls=%async_computation.5 | async-start | bytes 2621440 | tf_op jit(solution)/shard_map/all_gather | solution.py:72
  89.2 41.2 %copy-start.12 = (f32[1,256]{1,0:T(1,128)S(1)}, f32[1,256]{1,0:T(1,128)}, u32[]{:S(2)}) copy-start(f32[1,256]{1,0:T(1,128)} %param.25) | copy-start | bytes 3076
  130.3 41.0 %copy-start.13 = (f32[1,256]{1,0:T(1,128)S(1)}, f32[1,256]{1,0:T(1,128)}, u32[]{:S(2)}) copy-start(f32[1,256]{1,0:T(1,128)} %param.24) | copy-start | bytes 3076
  171.3 4.8 copy-start.1
  176.0 1.7 copy-start.2
  176.0 3.7 copy-start.4
  176.1 3.8 copy-start.5
  176.1 3.8 copy-start.7
  176.1 22.0 %copy-start.8 = (f32[1,256]{1,0:T(1,128)S(1)}, f32[1,256]{1,0:T(1,128)}, u32[]{:S(2)}) copy-start(f32[1,256]{1,0:T(1,128)} %param.35) | copy-start | bytes 3076
  176.1 148.6 %all-gather.22.cloned.1.call-start = ((), (), s32[]{:S(2)}) async-start(), calls=%async_computation.7 | async-start | bytes 6488064 | tf_op jit(solution)/shard_map/all_gather | solution.py:88
  177.1 1.6 copy-start.3
  177.2 240.2 %all-gather.24.cloned.1.call-start = ((), (), s32[]{:S(2)}) async-start(), calls=%async_computation.8 | async-start | bytes 6488064 | tf_op jit(solution)/shard_map/all_gather | solution.py:91
  178.7 332.1 %all-gather.26.cloned.1.call-start = ((), (), s32[]{:S(2)}) async-start(), calls=%async_computation.9 | async-start | bytes 6488064 | tf_op jit(solution)/shard_map/all_gather | solution.py:97
  179.7 394.8 %reduce-scatter.2.cloned.1.call-start = ((), (), s32[]{:S(2)}) async-start(), calls=%async_computation.10 | async-start | bytes 5242880 | tf_op jit(solution)/shard_map/reduce_scatter | solution.py:102
  230.2 94.5 %copy-start.10 = (f32[2048]{0:T(1024)S(1)}, f32[2048]{0:T(1024)}, u32[]{:S(2)}) copy-start(f32[2048]{0:T(1024)} %param.20) | copy-start | bytes 24580
Sparse Core Ops, SparseCore 0:
  8.9 37.1 all-gather.9
  48.2 40.8 all-gather.15
  91.3 38.9 all-gather.13
  132.3 38.9 all-gather.11
  172.7 33.1 all-gather.19
  207.3 22.8 all-gather.17
  232.3 92.2 all-gather.21
  326.9 90.4 all-gather.23
  419.4 91.2 all-gather.25
  531.9 42.5 reduce-scatter.1
